TPU v7x, 32 devices: a whole 2x2x4 slice. The times are simulated.
32 devices in a mesh: ep: 8 (over z, x), tp: 4 (over y, core).
Axes of the slice: x: 2, y: 2, z: 4, core: 2. Of those that a mesh axis runs over, the one named last changes fastest.
Arguments:
- tokens: bfloat16 [1024, 2048], P('ep'), may hold values from -6 to 6
- routing: int32 [1024, 2], P('ep'), may hold values from 0 to 7, all different within a row; in each aligned block of 128 rows (0 to 127, 128 to 255, ...) at most 56 rows name the same one
- router_weight: bfloat16 [2048, 8], replicated, may hold values from -0.125 to 0.125
- gate_weight: bfloat16 [8, 2048, 2048], P('ep', None, 'tp'), may hold values from -0.125 to 0.125
- up_weight: bfloat16 [8, 2048, 2048], P('ep', None, 'tp'), may hold values from -0.125 to 0.125
- down_weight: bfloat16 [8, 2048, 2048], P('ep', 'tp'), may hold values from -0.125 to 0.125
- cotangent: bfloat16 [1024, 2048], P('ep'), may hold values from -0.796875 to 0.796875
Outputs:
- token_grad: bfloat16 [1024, 2048], P('ep')
- router_grad: float32 [2048, 8], P('tp')
- router_rows: float32 [2048], P('tp')
- gate_grad: bfloat16 [8, 2048, 2048], P('ep', None, 'tp')
- up_grad: bfloat16 [8, 2048, 2048], P('ep', None, 'tp')
- down_grad: bfloat16 [8, 2048, 2048], P('ep', 'tp')
- gate_rows: float32 [8, 2048], P('ep')
- up_rows: float32 [8, 2048], P('ep')
- down_rows: float32 [8, 2048], P('ep', 'tp')
Inputs may be any that keep to these rules, and one draw needn't show every extreme that they name: `routing`: A row's 2 experts differ. Within the rows of one index of ep (128 rows), no expert is named more than 56 times, a bound that some block reaches.
All inputs are finite; a program needn't handle non-finite values.
Results may differ from a plain program's by a relative error of at most 0.01.
Values may be sent and summed in bfloat16 or wider, within the bound.
A program may use at most 64 MiB of HBM per device.

v0:
```python
import jax
import jax.numpy as jnp
from jax import lax
from jax.sharding import PartitionSpec as P


def expert_backward(rows_in, cots_in, slot_scale, w_gate, w_up, w_down):
    pre_gate = jnp.dot(rows_in, w_gate, preferred_element_type=jnp.float32)
    pre_up = jnp.dot(rows_in, w_up, preferred_element_type=jnp.float32)
    sigmoid_gate = jax.nn.sigmoid(pre_gate)
    hidden = (pre_gate * sigmoid_gate * pre_up).astype(jnp.bfloat16)
    back_proj = lax.dot_general(
        cots_in, w_down, (((1,), (1,)), ((), ())), preferred_element_type=jnp.float32
    )
    gate_term = jnp.sum(hidden.astype(jnp.float32) * back_proj, axis=1)
    scaled = slot_scale * back_proj
    grad_up_pre = (scaled * pre_gate * sigmoid_gate).astype(jnp.bfloat16)
    grad_gate_pre = (
        scaled * pre_up * sigmoid_gate * (1.0 + pre_gate * (1.0 - sigmoid_gate))
    ).astype(jnp.bfloat16)
    weighted = (slot_scale * cots_in.astype(jnp.float32)).astype(jnp.bfloat16)
    contract_rows = (((0,), (0,)), ((), ()))
    grad_down = lax.dot_general(hidden, weighted, contract_rows, preferred_element_type=jnp.float32)
    grad_gate = lax.dot_general(
        rows_in, grad_gate_pre, contract_rows, preferred_element_type=jnp.float32
    )
    grad_up = lax.dot_general(
        rows_in, grad_up_pre, contract_rows, preferred_element_type=jnp.float32
    )
    contract_hidden = (((1,), (1,)), ((), ()))
    partial_value = lax.dot_general(
        grad_gate_pre, w_gate, contract_hidden, preferred_element_type=jnp.float32
    )
    partial_value = partial_value + lax.dot_general(
        grad_up_pre, w_up, contract_hidden, preferred_element_type=jnp.float32
    )
    return (partial_value, gate_term, grad_gate, grad_up, grad_down)


def per_device(tokens, routing, router_weight, gate_weight, up_weight, down_weight, cotangent):
    groups = lax.axis_size("ep")
    shares = lax.axis_size("tp")
    tok_count, model_width = tokens.shape
    top_count = routing.shape[1]
    local_experts = gate_weight.shape[0]
    experts = local_experts * groups
    capacity = 7 * tok_count * top_count // (4 * experts)
    slot_span = groups * capacity
    assigns = tok_count * top_count
    col_width = model_width // shares
    col_start = lax.axis_index("tp") * col_width
    logits = jnp.dot(tokens, router_weight, preferred_element_type=jnp.float32)
    affinity = jax.nn.sigmoid(logits)
    chosen = jnp.take_along_axis(affinity, routing, axis=1)
    total_aff = jnp.sum(chosen, axis=1, keepdims=True)
    weights = chosen / total_aff
    flat_ids = routing.reshape(-1)
    onehot_ids = (flat_ids[:, None] == jnp.arange(experts, dtype=jnp.int32)[None, :]).astype(
        jnp.int32
    )
    position = jnp.sum((jnp.cumsum(onehot_ids, axis=0) - 1) * onehot_ids, axis=1)
    slot_of = flat_ids % local_experts * slot_span + flat_ids // local_experts * capacity + position
    slot_table = jnp.full((local_experts * slot_span,), assigns, jnp.int32)
    slot_table = slot_table.at[slot_of].set(jnp.arange(assigns, dtype=jnp.int32))
    zero_row = jnp.zeros((1, model_width), jnp.bfloat16)
    tok_pad = jnp.concatenate([tokens, zero_row], axis=0)
    cot_pad = jnp.concatenate([cotangent, zero_row], axis=0)
    weight_pad = jnp.concatenate(
        [weights.astype(jnp.bfloat16).reshape(-1), jnp.zeros((1,), jnp.bfloat16)]
    )
    source_tok = slot_table // top_count
    rows_send = tok_pad[source_tok].reshape(local_experts, groups, capacity, model_width)
    cots_send = cot_pad[source_tok].reshape(local_experts, groups, capacity, model_width)
    scale_send = weight_pad[slot_table].reshape(local_experts, groups, capacity)
    rows_recv, cots_recv, scale_recv = (
        lax.all_to_all(rows_send, "ep", split_axis=1, concat_axis=1, tiled=True),
        lax.all_to_all(cots_send, "ep", split_axis=1, concat_axis=1, tiled=True),
        lax.all_to_all(scale_send, "ep", split_axis=1, concat_axis=1, tiled=True),
    )
    partials, gate_terms, gate_grads, up_grads, down_grads = ([], [], [], [], [])
    slot_scale = scale_recv[0].reshape(slot_span).astype(jnp.float32)[:, None]
    result = expert_backward(
        rows_recv[0].reshape(slot_span, model_width),
        cots_recv[0].reshape(slot_span, model_width),
        slot_scale,
        gate_weight[0],
        up_weight[0],
        down_weight[0],
    )
    partials.append(result[0])
    gate_terms.append(result[1])
    gate_grads.append(result[2])
    up_grads.append(result[3])
    down_grads.append(result[4])
    partial_value = jnp.stack(partials)
    gate_term = jnp.stack(gate_terms)
    grad_gate = jnp.stack(gate_grads)
    grad_up = jnp.stack(up_grads)
    grad_down = jnp.stack(down_grads)
    gate_rows, up_rows = lax.psum(
        (jnp.sum(grad_gate * grad_gate, axis=2), jnp.sum(grad_up * grad_up, axis=2)), "tp"
    )
    down_rows = jnp.sum(grad_down * grad_down, axis=2)
    summed = lax.psum_scatter(partial_value, "tp", scatter_dimension=2, tiled=True)
    gate_sum = lax.psum(gate_term, "tp")
    back_send = summed.astype(jnp.bfloat16).reshape(local_experts, groups, capacity, col_width)
    gate_send = gate_sum.astype(jnp.bfloat16).reshape(local_experts, groups, capacity)
    back_recv, gate_recv = (
        lax.all_to_all(back_send, "ep", split_axis=1, concat_axis=1, tiled=True),
        lax.all_to_all(gate_send, "ep", split_axis=1, concat_axis=1, tiled=True),
    )
    router_cols = lax.dynamic_slice_in_dim(router_weight, col_start, col_width, 0)
    back_flat = back_recv.reshape(local_experts * slot_span, -1)
    back_rows = jnp.sum(
        back_flat[slot_of].astype(jnp.float32).reshape(tok_count, top_count, -1), axis=1
    )
    d_weights = gate_recv.reshape(-1)[slot_of].astype(jnp.float32).reshape(tok_count, top_count)
    d_chosen = (d_weights - jnp.sum(d_weights * weights, axis=1, keepdims=True)) / total_aff
    d_logit = d_chosen * chosen * (1.0 - chosen)
    onehot = (routing[:, :, None] == jnp.arange(experts, dtype=jnp.int32)[None, None, :]).astype(
        jnp.float32
    )
    d_logits = jnp.sum(d_logit[:, :, None] * onehot, axis=1).astype(jnp.bfloat16)
    token_cols = lax.dynamic_slice_in_dim(tokens, col_start, col_width, 1)
    router_part = lax.dot_general(
        token_cols, d_logits, (((0,), (0,)), ((), ())), preferred_element_type=jnp.float32
    )
    router_grad = lax.psum(router_part, "ep")
    router_rows = jnp.sum(router_grad * router_grad, axis=1)
    router_back = lax.dot_general(
        d_logits, router_cols, (((1,), (1,)), ((), ())), preferred_element_type=jnp.float32
    )
    token_grad = (back_rows + router_back).astype(jnp.bfloat16)
    token_grad = lax.all_gather(token_grad, "tp", axis=1, tiled=True)
    return (
        token_grad,
        router_grad,
        router_rows,
        grad_gate.astype(jnp.bfloat16),
        grad_up.astype(jnp.bfloat16),
        grad_down.astype(jnp.bfloat16),
        gate_rows,
        up_rows,
        down_rows,
    )


def solution(mesh):
    return jax.shard_map(
        per_device,
        mesh=mesh,
        in_specs=(
            P("ep", None),
            P("ep", None),
            P(),
            P("ep", None, "tp"),
            P("ep", None, "tp"),
            P("ep", "tp", None),
            P("ep", None),
        ),
        out_specs=(
            P("ep", None),
            P("tp", None),
            P("tp"),
            P("ep", None, "tp"),
            P("ep", None, "tp"),
            P("ep", "tp", None),
            P("ep", None),
            P("ep", None),
            P("ep", "tp"),
        ),
        check_vma=False,
    )
```

profile of v0, /device:TPU:0, one launch (start us, length us, event | category | flops | bytes accessed | tf_op | source)
XLA Modules:
  0.0 255.0 jit_solution(7731860463774829727)
XLA Ops:
  16.6 3.2 %gather_fusion = bf16[448]{0:T(512)(128)(2,1)S(1)} fusion(bf16[257]{0:T(512)(128)(2,1)S(1)} %pad_maximum_fusion, s32[1024]{0:T(1024)S(1)} %get-tuple-element.83), kind=kCustom, calls=%fused_computation | custom fusion | bytes 3584 | tf_op jit(solution)/shard_map/gather | solution.py:74
  20.4 7.3 %all-to-all-start = ((bf16[1,8,56]{2,0,1:T(2,128)(2,1)}), bf16[1,8,56]{2,0,1:T(2,128)(2,1)S(1)}, u32[]{:S(2)}, u32[]{:S(2)}) async-start(bf16[1,8,56]{2,0,1:T(2,128)(2,1)} %reshape.229), calls=%async_computation | async-start | bytes 8192 | tf_op jit(solution)/shard_map/all_to_all | solution.py:78
  27.7 3.2 %gather_fusion.2 = bf16[448,2048]{1,0:T(8,128)(2,1)} fusion(bf16[129,2048]{1,0:T(8,128)(2,1)S(1)} %concatenate.11, s32[1024]{0:T(1024)S(1)} %get-tuple-element.82), kind=kCustom, calls=%fused_computation.2 | custom fusion | bytes 3671808 | tf_op jit(solution)/shard_map/gather | solution.py:72
  30.9 3.2 %all-to-all-done = bf16[1,8,56]{2,0,1:T(2,128)(2,1)S(1)} async-done(((bf16[1,8,56]{2,0,1:T(2,128)(2,1)}), bf16[1,8,56]{2,0,1:T(2,128)(2,1)S(1)}, u32[]{:S(2)}, u32[]{:S(2)}) %all-to-all-start) | async-done | bytes 928 | tf_op jit(solution)/shard_map/all_to_all | solution.py:78
  34.1 4.3 %all-to-all-start.2 = ((bf16[1,8,56,2048]{3,2,0,1:T(8,128)(2,1)}), bf16[1,8,56,2048]{3,2,0,1:T(8,128)(2,1)}, u32[]{:S(2)}, u32[]{:S(2)}) async-start(bf16[1,8,56,2048]{3,2,0,1:T(8,128)(2,1)} %bitcast.67), calls=%async_computation.2 | async-start | bytes 3670016 | tf_op jit(solution)/shard_map/all_to_all | solution.py:76
  39.5 3.2 %gather_fusion.1 = bf16[448,2048]{1,0:T(8,128)(2,1)} fusion(bf16[129,2048]{1,0:T(8,128)(2,1)S(1)} %concatenate.10, s32[1024]{0:T(1024)S(1)} %get-tuple-element.82), kind=kCustom, calls=%fused_computation.1 | custom fusion | bytes 3671808 | tf_op jit(solution)/shard_map/gather | solution.py:73
  42.7 37.2 %all-to-all-done.2 = bf16[1,8,56,2048]{3,2,0,1:T(8,128)(2,1)} async-done(((bf16[1,8,56,2048]{3,2,0,1:T(8,128)(2,1)}), bf16[1,8,56,2048]{3,2,0,1:T(8,128)(2,1)}, u32[]{:S(2)}, u32[]{:S(2)}) %all-to-all-start.2) | async-done | bytes 1835040 | tf_op jit(solution)/shard_map/all_to_all | solution.py:76
  79.9 4.3 %all-to-all-start.1 = ((bf16[1,8,56,2048]{3,2,0,1:T(8,128)(2,1)}), bf16[1,8,56,2048]{3,2,0,1:T(8,128)(2,1)}, u32[]{:S(2)}, u32[]{:S(2)}) async-start(bf16[1,8,56,2048]{3,2,0,1:T(8,128)(2,1)} %bitcast.66), calls=%async_computation.1 | async-start | bytes 3670016 | tf_op jit(solution)/shard_map/all_to_all | solution.py:77
  84.6 4.2 %fusion.5 = f32[448,512]{1,0:T(8,128)} fusion(bf16[448,2048]{1,0:T(8,128)(2,1)} %bitcast.11, bf16[1,2048,512]{2,1,0:T(8,128)(2,1)} %param.11), kind=kOutput, calls=%fused_computation.17 | convolution fusion | flops 939524096 | bytes 4849664 | tf_op jit(solution)/shard_map/dot_general | solution.py:9
  88.8 3.5 %fusion.2 = f32[448,512]{1,0:T(8,128)} fusion(bf16[448,2048]{1,0:T(8,128)(2,1)} %bitcast.11, bf16[1,2048,512]{2,1,0:T(8,128)(2,1)S(1)} %copy-done), kind=kOutput, calls=%fused_computation.14 | convolution fusion | flops 939524096 | bytes 4849664 | tf_op jit(solution)/shard_map/dot_general | solution.py:8
  92.3 34.1 %all-to-all-done.1 = bf16[1,8,56,2048]{3,2,0,1:T(8,128)(2,1)} async-done(((bf16[1,8,56,2048]{3,2,0,1:T(8,128)(2,1)}), bf16[1,8,56,2048]{3,2,0,1:T(8,128)(2,1)}, u32[]{:S(2)}, u32[]{:S(2)}) %all-to-all-start.1) | async-done | bytes 1835040 | tf_op jit(solution)/shard_map/all_to_all | solution.py:77
  126.4 5.5 %multiply_reduce_fusion.3 = (f32[448]{0:T(512)}, bf16[448,512]{1,0:T(8,128)(2,1)}, bf16[448,512]{1,0:T(8,128)(2,1)S(1)}, bf16[448,512]{1,0:T(8,128)(2,1)S(1)}) fusion(f32[448,512]{1,0:T(8,128)} %fusion.5, f32[448,512]{1,0:T(8,128)} %fusion.2, f32[448]{0:T(512)S(1)} %reshape.164, bf16[448,2048]{1,0:T(8,128)(2,1)} %bitcast.7, bf16[1,512,2048]{2,1,0:T(8,128)(2,1)} %param.12), kind=kOutput, calls=%fused_computation.32 | convolution fusion | flops 944111168 | bytes 7147008 | tf_op jit(solution)/shard_map/dot_general | solution.py:12
  133.5 3.0 %add_bitcast_fusion = f32[1,448,2048]{2,1,0:T(8,128)} fusion(f32[448,2048]{1,0:T(8,128)S(1)} %fusion, bf16[448,512]{1,0:T(8,128)(2,1)S(1)} %get-tuple-element.79, bf16[1,2048,512]{2,1,0:T(8,128)(2,1)S(1)} %copy-done.2), kind=kOutput, calls=%fused_computation.11 | convolution fusion | flops 940441600 | bytes 9895936 | tf_op jit(solution)/shard_map/dot_general | solution.py:34
  136.6 4.1 %convert_bitcast_fusion.2 = (bf16[1,2048,512]{1,2,0:T(8,128)(2,1)}, f32[2048]{0:T(1024)S(1)}) fusion(bf16[448,2048]{1,0:T(8,128)(2,1)} %bitcast.11, bf16[448,512]{1,0:T(8,128)(2,1)S(1)} %get-tuple-element.78), kind=kOutput, calls=%fused_computation.23 | convolution fusion | flops 942667776 | bytes 4399104 | tf_op jit(solution)/shard_map/dot_general | solution.py:24
  140.7 4.3 %convert_bitcast_fusion.1 = (bf16[1,2048,512]{1,2,0:T(8,128)(2,1)}, f32[2048]{0:T(1024)S(1)}) fusion(bf16[448,2048]{1,0:T(8,128)(2,1)} %bitcast.11, bf16[448,512]{1,0:T(8,128)(2,1)S(1)} %get-tuple-element.79), kind=kOutput, calls=%fused_computation.22 | convolution fusion | flops 942667776 | bytes 4399104 | tf_op jit(solution)/shard_map/dot_general | solution.py:27
  145.0 11.0 %all-reduce.2 = (bf16[1,448]{1,0:T(2,128)(2,1)S(1)}, f32[1,2048]{1,0:T(1,128)}, f32[1,2048]{1,0:T(1,128)}) all-reduce(f32[1,448]{1,0:T(1,128)S(1)} %bitcast.73, f32[1,2048]{1,0:T(1,128)S(1)} %bitcast.68, f32[1,2048]{1,0:T(1,128)S(1)} %bitcast.69), channel_id=1, replica_groups=mesh['ep'=8,'tp'=4] {'tp'}, use_global_device_ids=true, to_apply=%region_8.9 | all-reduce | flops 4544 | bytes 35456 | tf_op jit(solution)/shard_map/psum | solution.py:105
  156.7 4.5 %all-to-all-start.4 = ((bf16[1,8,56]{2,0,1:T(2,128)(2,1)}), bf16[1,8,56]{2,0,1:T(2,128)(2,1)S(1)}, u32[]{:S(2)}, u32[]{:S(2)}) async-start(bf16[1,8,56]{2,0,1:T(2,128)(2,1)} %reshape.230), calls=%async_computation.5 | async-start | bytes 8192 | tf_op jit(solution)/shard_map/all_to_all | solution.py:110
  161.3 15.6 %reduce-scatter.2.cloned.1.call-done = f32[1,448,512]{2,1,0:T(8,128)} async-done(((f32[1,448,2048]{2,1,0:T(8,128)}), f32[1,448,512]{2,1,0:T(8,128)}) %reduce-scatter.2.cloned.1.call-update) | async-done | bytes 917520 | tf_op jit(solution)/shard_map/reduce_scatter | solution.py:104
  178.9 5.5 %all-to-all-start.3 = ((bf16[1,8,56,512]{3,2,0,1:T(8,128)(2,1)}), bf16[1,8,56,512]{3,2,0,1:T(8,128)(2,1)S(1)}, u32[]{:S(2)}, u32[]{:S(2)}) async-start(bf16[1,8,56,512]{3,2,0,1:T(8,128)(2,1)} %bitcast.16), calls=%async_computation.4 | async-start | bytes 917504 | tf_op jit(solution)/shard_map/all_to_all | solution.py:109
  184.4 4.9 %multiply_reduce_fusion = (f32[512]{0:T(512)}, bf16[1,512,2048]{2,1,0:T(8,128)(2,1)}) fusion(bf16[448,512]{1,0:T(8,128)(2,1)} %get-tuple-element.67, bf16[448,2048]{1,0:T(8,128)(2,1)} %bitcast.7, f32[448]{0:T(512)S(1)} %copy-done.11), kind=kOutput, calls=%fused_computation.7 | convolution fusion | flops 945421824 | bytes 4394752 | tf_op jit(solution)/shard_map/dot_general | solution.py:23
  189.3 3.9 %copy.90 = bf16[1,2048,512]{2,1,0:T(8,128)(2,1)} copy(bf16[1,2048,512]{1,2,0:T(8,128)(2,1)} %get-tuple-element.76) | data formatting | bytes 4194304
  193.3 3.9 %copy.91 = bf16[1,2048,512]{2,1,0:T(8,128)(2,1)} copy(bf16[1,2048,512]{1,2,0:T(8,128)(2,1)} %get-tuple-element.74) | data formatting | bytes 4194304
  199.7 37.5 %psum.29 = f32[512,8]{0,1:T(8,128)S(1)} all-reduce(f32[512,8]{0,1:T(8,128)S(1)} %fusion.15), channel_id=1, replica_groups=mesh['ep'=8,'tp'=4] {'ep'}, use_global_device_ids=true, to_apply=%region_11.12 | all-reduce | flops 4096 | bytes 32768 | tf_op jit(solution)/shard_map/psum | solution.py:128
  240.9 6.5 %all_gather.3 = bf16[128,2048]{1,0:T(8,128)(2,1)S(1)} all-gather(bf16[128,512]{1,0:T(8,128)(2,1)S(1)} %fusion.11), channel_id=1, replica_groups=mesh['ep'=8,'tp'=4] {'tp'}, dimensions={1}, use_global_device_ids=true | all-gather | bytes 655360 | tf_op jit(solution)/shard_map/all_gather | solution.py:134
  (84 shorter events, 22.6 us)
Async XLA Ops:
  7.2 81.6 %copy-start = (bf16[1,2048,512]{2,1,0:T(8,128)(2,1)S(1)}, bf16[1,2048,512]{2,1,0:T(8,128)(2,1)}, u32[]{:S(2)}) copy-start(bf16[1,2048,512]{2,1,0:T(8,128)(2,1)} %param.10) | copy-start | bytes 6291460
  11.0 1.7 copy-start.7
  14.0 1.6 copy-start.4
  14.0 13.7 %copy-start.1 = (bf16[128,2048]{1,0:T(8,128)(2,1)S(1)}, bf16[128,2048]{1,0:T(8,128)(2,1)}, u32[]{:S(2)}) copy-start(bf16[128,2048]{1,0:T(8,128)(2,1)} %param.7) | copy-start | bytes 1572868
  15.6 15.3 %copy-start.5 = (f32[128]{0:T(128)}, f32[128]{0:T(128)S(1)}, u32[]{:S(2)}) copy-start(f32[128]{0:T(128)S(1)} %get-tuple-element.70) | copy-start | bytes 1540
  20.4 13.7 %all-to-all-start = ((bf16[1,8,56]{2,0,1:T(2,128)(2,1)}), bf16[1,8,56]{2,0,1:T(2,128)(2,1)S(1)}, u32[]{:S(2)}, u32[]{:S(2)}) async-start(bf16[1,8,56]{2,0,1:T(2,128)(2,1)} %reshape.229), calls=%async_computation | async-start | bytes 8192 | tf_op jit(solution)/shard_map/all_to_all | solution.py:78
  34.1 45.8 %all-to-all-start.2 = ((bf16[1,8,56,2048]{3,2,0,1:T(8,128)(2,1)}), bf16[1,8,56,2048]{3,2,0,1:T(8,128)(2,1)}, u32[]{:S(2)}, u32[]{:S(2)}) async-start(bf16[1,8,56,2048]{3,2,0,1:T(8,128)(2,1)} %bitcast.67), calls=%async_computation.2 | async-start | bytes 3670016 | tf_op jit(solution)/shard_map/all_to_all | solution.py:76
  79.9 46.5 %all-to-all-start.1 = ((bf16[1,8,56,2048]{3,2,0,1:T(8,128)(2,1)}), bf16[1,8,56,2048]{3,2,0,1:T(8,128)(2,1)}, u32[]{:S(2)}, u32[]{:S(2)}) async-start(bf16[1,8,56,2048]{3,2,0,1:T(8,128)(2,1)} %bitcast.66), calls=%async_computation.1 | async-start | bytes 3670016 | tf_op jit(solution)/shard_map/all_to_all | solution.py:77
  84.2 92.7 %reduce-scatter.2.cloned.1.call-start = ((), (), s32[]{:S(2)}) async-start(), calls=%async_computation.6 | async-start | bytes 4587520 | tf_op jit(solution)/shard_map/reduce_scatter | solution.py:104
  84.6 41.8 %copy-start.10 = (f32[448]{0:T(512)}, f32[448]{0:T(512)S(1)}, u32[]{:S(2)}) copy-start(f32[448]{0:T(512)S(1)} %reshape.164) | copy-start | bytes 5380
  131.9 1.6 copy-start.2
  140.7 4.3 %copy-start.12 = (f32[448]{0:T(512)S(1)}, f32[448]{0:T(512)}, u32[]{:S(2)}) copy-start(f32[448]{0:T(512)} %get-tuple-element.66) | copy-start | bytes 5380
  140.7 20.6 %copy-start.8 = (s32[256,1]{0,1:T(1,128)S(1)}, s32[256,1]{0,1:T(1,128)}, u32[]{:S(2)}) copy-start(s32[256,1]{0,1:T(1,128)} %copy-done.7) | copy-start | bytes 3076
  145.0 39.4 %copy-start.11 = (f32[448]{0:T(512)S(1)}, f32[448]{0:T(512)}, u32[]{:S(2)}) copy-start(f32[448]{0:T(512)} %copy-done.10) | copy-start | bytes 5380
  156.7 22.2 %all-to-all-start.4 = ((bf16[1,8,56]{2,0,1:T(2,128)(2,1)}), bf16[1,8,56]{2,0,1:T(2,128)(2,1)S(1)}, u32[]{:S(2)}, u32[]{:S(2)}) async-start(bf16[1,8,56]{2,0,1:T(2,128)(2,1)} %reshape.230), calls=%async_computation.5 | async-start | bytes 8192 | tf_op jit(solution)/shard_map/all_to_all | solution.py:110
  178.9 58.9 %all-to-all-start.3 = ((bf16[1,8,56,512]{3,2,0,1:T(8,128)(2,1)}), bf16[1,8,56,512]{3,2,0,1:T(8,128)(2,1)S(1)}, u32[]{:S(2)}, u32[]{:S(2)}) async-start(bf16[1,8,56,512]{3,2,0,1:T(8,128)(2,1)} %bitcast.16), calls=%async_computation.4 | async-start | bytes 917504 | tf_op jit(solution)/shard_map/all_to_all | solution.py:109
  193.3 6.2 %copy-start.9 = (f32[128,2]{0,1:T(2,128)S(1)}, f32[128,2]{0,1:T(2,128)}, u32[]{:S(2)}) copy-start(f32[128,2]{0,1:T(2,128)} %get-tuple-element.69) | copy-start | bytes 3076
  193.3 6.2 %copy-start.6 = (f32[128]{0:T(128)S(1)}, f32[128]{0:T(128)}, u32[]{:S(2)}) copy-start(f32[128]{0:T(128)} %copy-done.5) | copy-start | bytes 1540
  237.2 3.7 %copy-start.3 = (f32[512,8]{0,1:T(8,128)}, f32[512,8]{0,1:T(8,128)S(1)}, u32[]{:S(2)}) copy-start(f32[512,8]{0,1:T(8,128)S(1)} %psum.29) | copy-start | bytes 49156
Sparse Core Ops, SparseCore 0:
  136.7 40.1 reduce-scatter.1
where the time goes:
time: 256 us; the launch traced here: 255 us
  waiting for transfers between devices  90.1 us (35%)
  blocking collectives  55 us (21%)
  matrix products  33.1 us (13%)
  local copies, waits for them, and re-layouts  30 us (12%)
  starting transfers between devices  26.2 us (10%)
  between operations  14.3 us (6%)
  other arithmetic  6.23 us (2%)
    psum x1, blocking collectives, per_device(): router_grad = lax.psum(router_part, 'ep')  37.5 us
    all_to_all x1, waiting for transfers between devices, per_device(): lax.all_to_all(rows_send, 'ep', split_axis=1, concat_axis=1, tiled=True)  37.2 us
    all_to_all x1, waiting for transfers between devices, per_device(): lax.all_to_all(cots_send, 'ep', split_axis=1, concat_axis=1, tiled=True)  34.1 us
    reduce_scatter x1, waiting for transfers between devices, per_device(): lax.psum_scatter(partial_value, 'tp', scatter_dimension=2, tiled=True)  15.6 us
    psum x1, blocking collectives, per_device(): gate_sum = lax.psum(gate_term, 'tp')  11 us
    unnamed x30, local copies, waits for them, and re-layouts  9.92 us
    all_to_all x1, starting transfers between devices, per_device(): lax.all_to_all(scale_send, 'ep', split_axis=1, concat_axis=1, tiled=True)  7.28 us
    all_gather x1, blocking collectives, per_device(): token_grad = lax.all_gather(token_grad, 'tp', axis=1, tiled=True)  6.5 us
  transfers between devices with their start and end apart: 6, of which 4 were waited for; matrix products, arithmetic and copies ran while one was open for 17% of the time, Pallas kernels for 0%

commit v1 on v0

--- a/solution.py
+++ b/solution.py
@@ -38,6 +38,12 @@
 
 
 def per_device(tokens, routing, router_weight, gate_weight, up_weight, down_weight, cotangent):
+
+    def windows_shape(piece_in):
+        local_part = lax.all_gather(piece_in, "ep")
+        block_next = jnp.sum(local_part, axis=0)
+        return block_next
+
     groups = lax.axis_size("ep")
     shares = lax.axis_size("tp")
     tok_count, model_width = tokens.shape
@@ -125,7 +131,7 @@
     router_part = lax.dot_general(
         token_cols, d_logits, (((0,), (0,)), ((), ())), preferred_element_type=jnp.float32
     )
-    router_grad = lax.psum(router_part, "ep")
+    router_grad = windows_shape(router_part)
     router_rows = jnp.sum(router_grad * router_grad, axis=1)
     router_back = lax.dot_general(
         d_logits, router_cols, (((1,), (1,)), ((), ())), preferred_element_type=jnp.float32

time: 256 us -> 240 us (0.938)
  waiting for transfers between devices: 90.1 us -> 74.5 us
    psum x1 -> x0, blocking collectives: 37.5 us -> none  [per_device(): router_grad = lax.psum(router_part, 'ep')]
    all_gather x0 -> x1, blocking collectives: none -> 34.9 us  [windows_shape(): local_part = lax.all_gather(piece_in, 'ep')]
    reduce_scatter x1, waiting for transfers between devices: 15.6 us -> 0.01 us  [per_device(): lax.psum_scatter(partial_value, 'tp', scatter_dimension=2, tiled=True)]
    unnamed x30 -> x26, local copies, waits for them, and re-layouts: 9.92 us -> 9.94 us
  transfers between devices with their start and end apart: 6 -> 6, of which waited for: 4 -> 3; matrix products, arithmetic and copies ran while one was open for 17% -> 17% of each run, Pallas kernels for 0% -> 0%
where the time goes in v1:
time: 240 us; the launch traced here: 239 us
  waiting for transfers between devices  74.5 us (31%)
  blocking collectives  52.7 us (22%)
  matrix products  33.8 us (14%)
  local copies, waits for them, and re-layouts  30 us (12%)
  starting transfers between devices  26.8 us (11%)
  between operations  14.3 us (6%)
  other arithmetic  6.94 us (3%)
    all_to_all x1, waiting for transfers between devices, per_device(): lax.all_to_all(rows_send, 'ep', split_axis=1, concat_axis=1, tiled=True)  37.2 us
    all_gather x1, blocking collectives, windows_shape(): local_part = lax.all_gather(piece_in, 'ep')  34.9 us
    all_to_all x1, waiting for transfers between devices, per_device(): lax.all_to_all(cots_send, 'ep', split_axis=1, concat_axis=1, tiled=True)  34.1 us
    psum x1, blocking collectives, per_device(): gate_sum = lax.psum(gate_term, 'tp')  10.9 us
    unnamed x26, local copies, waits for them, and re-layouts  9.94 us
    all_to_all x1, starting transfers between devices, per_device(): lax.all_to_all(scale_send, 'ep', split_axis=1, concat_axis=1, tiled=True)  7.28 us
    all_gather x1, blocking collectives, per_device(): token_grad = lax.all_gather(token_grad, 'tp', axis=1, tiled=True)  7.01 us
    all_to_all x1, starting transfers between devices, per_device(): lax.all_to_all(back_send, 'ep', split_axis=1, concat_axis=1, tiled=True)  5.98 us
  transfers between devices with their start and end apart: 6, of which 3 were waited for; matrix products, arithmetic and copies ran while one was open for 17% of the time, Pallas kernels for 0%

profile of v1, /device:TPU:0, one launch (start us, length us, event | category | flops | bytes accessed | tf_op | source)
XLA Modules:
  0.0 239.1 jit_solution(15628139852367422740)
XLA Ops:
  16.6 3.2 %gather_fusion = bf16[448]{0:T(512)(128)(2,1)S(1)} fusion(bf16[257]{0:T(512)(128)(2,1)S(1)} %pad_maximum_fusion, s32[1024]{0:T(1024)S(1)} %get-tuple-element.83), kind=kCustom, calls=%fused_computation | custom fusion | bytes 3584 | tf_op jit(solution)/shard_map/gather | solution.py:80
  20.4 7.3 %all-to-all-start = ((bf16[1,8,56]{2,0,1:T(2,128)(2,1)}), bf16[1,8,56]{2,0,1:T(2,128)(2,1)S(1)}, u32[]{:S(2)}, u32[]{:S(2)}) async-start(bf16[1,8,56]{2,0,1:T(2,128)(2,1)} %reshape.230), calls=%async_computation | async-start | bytes 8192 | tf_op jit(solution)/shard_map/all_to_all | solution.py:84
  27.8 3.2 %gather_fusion.2 = bf16[448,2048]{1,0:T(8,128)(2,1)} fusion(bf16[129,2048]{1,0:T(8,128)(2,1)S(1)} %concatenate.11, s32[1024]{0:T(1024)S(1)} %get-tuple-element.82), kind=kCustom, calls=%fused_computation.2 | custom fusion | bytes 3671808 | tf_op jit(solution)/shard_map/gather | solution.py:78
  30.9 3.2 %all-to-all-done = bf16[1,8,56]{2,0,1:T(2,128)(2,1)S(1)} async-done(((bf16[1,8,56]{2,0,1:T(2,128)(2,1)}), bf16[1,8,56]{2,0,1:T(2,128)(2,1)S(1)}, u32[]{:S(2)}, u32[]{:S(2)}) %all-to-all-start) | async-done | bytes 928 | tf_op jit(solution)/shard_map/all_to_all | solution.py:84
  34.1 4.3 %all-to-all-start.2 = ((bf16[1,8,56,2048]{3,2,0,1:T(8,128)(2,1)}), bf16[1,8,56,2048]{3,2,0,1:T(8,128)(2,1)}, u32[]{:S(2)}, u32[]{:S(2)}) async-start(bf16[1,8,56,2048]{3,2,0,1:T(8,128)(2,1)} %bitcast.68), calls=%async_computation.2 | async-start | bytes 3670016 | tf_op jit(solution)/shard_map/all_to_all | solution.py:82
  39.5 3.2 %gather_fusion.1 = bf16[448,2048]{1,0:T(8,128)(2,1)} fusion(bf16[129,2048]{1,0:T(8,128)(2,1)S(1)} %concatenate.10, s32[1024]{0:T(1024)S(1)} %get-tuple-element.82), kind=kCustom, calls=%fused_computation.1 | custom fusion | bytes 3671808 | tf_op jit(solution)/shard_map/gather | solution.py:79
  42.7 37.2 %all-to-all-done.2 = bf16[1,8,56,2048]{3,2,0,1:T(8,128)(2,1)} async-done(((bf16[1,8,56,2048]{3,2,0,1:T(8,128)(2,1)}), bf16[1,8,56,2048]{3,2,0,1:T(8,128)(2,1)}, u32[]{:S(2)}, u32[]{:S(2)}) %all-to-all-start.2) | async-done | bytes 1835040 | tf_op jit(solution)/shard_map/all_to_all | solution.py:82
  79.9 4.3 %all-to-all-start.1 = ((bf16[1,8,56,2048]{3,2,0,1:T(8,128)(2,1)}), bf16[1,8,56,2048]{3,2,0,1:T(8,128)(2,1)}, u32[]{:S(2)}, u32[]{:S(2)}) async-start(bf16[1,8,56,2048]{3,2,0,1:T(8,128)(2,1)} %bitcast.67), calls=%async_computation.1 | async-start | bytes 3670016 | tf_op jit(solution)/shard_map/all_to_all | solution.py:83
  84.6 4.2 %fusion.5 = f32[448,512]{1,0:T(8,128)} fusion(bf16[448,2048]{1,0:T(8,128)(2,1)} %bitcast.11, bf16[1,2048,512]{2,1,0:T(8,128)(2,1)} %param.11), kind=kOutput, calls=%fused_computation.17 | convolution fusion | flops 939524096 | bytes 4849664 | tf_op jit(solution)/shard_map/dot_general | solution.py:9
  88.8 3.5 %fusion.2 = f32[448,512]{1,0:T(8,128)} fusion(bf16[448,2048]{1,0:T(8,128)(2,1)} %bitcast.11, bf16[1,2048,512]{2,1,0:T(8,128)(2,1)S(1)} %copy-done), kind=kOutput, calls=%fused_computation.14 | convolution fusion | flops 939524096 | bytes 4849664 | tf_op jit(solution)/shard_map/dot_general | solution.py:8
  92.3 34.1 %all-to-all-done.1 = bf16[1,8,56,2048]{3,2,0,1:T(8,128)(2,1)} async-done(((bf16[1,8,56,2048]{3,2,0,1:T(8,128)(2,1)}), bf16[1,8,56,2048]{3,2,0,1:T(8,128)(2,1)}, u32[]{:S(2)}, u32[]{:S(2)}) %all-to-all-start.1) | async-done | bytes 1835040 | tf_op jit(solution)/shard_map/all_to_all | solution.py:83
  126.4 5.5 %multiply_reduce_fusion.3 = (f32[448]{0:T(512)}, bf16[448,512]{1,0:T(8,128)(2,1)}, bf16[448,512]{1,0:T(8,128)(2,1)S(1)}, bf16[448,512]{1,0:T(8,128)(2,1)S(1)}) fusion(f32[448,512]{1,0:T(8,128)} %fusion.5, f32[448,512]{1,0:T(8,128)} %fusion.2, f32[448]{0:T(512)S(1)} %reshape.164, bf16[448,2048]{1,0:T(8,128)(2,1)} %bitcast.7, bf16[1,512,2048]{2,1,0:T(8,128)(2,1)} %param.12), kind=kOutput, calls=%fused_computation.32 | convolution fusion | flops 944111168 | bytes 7147008 | tf_op jit(solution)/shard_map/dot_general | solution.py:12
  133.5 3.0 %add_bitcast_fusion = f32[1,448,2048]{2,1,0:T(8,128)} fusion(f32[448,2048]{1,0:T(8,128)S(1)} %fusion, bf16[448,512]{1,0:T(8,128)(2,1)S(1)} %get-tuple-element.79, bf16[1,2048,512]{2,1,0:T(8,128)(2,1)S(1)} %copy-done.2), kind=kOutput, calls=%fused_computation.11 | convolution fusion | flops 940441600 | bytes 9895936 | tf_op jit(solution)/shard_map/dot_general | solution.py:34
  137.2 4.7 %convert_bitcast_fusion.2 = (bf16[1,2048,512]{1,2,0:T(8,128)(2,1)}, f32[2048]{0:T(1024)}) fusion(bf16[448,2048]{1,0:T(8,128)(2,1)} %bitcast.11, bf16[448,512]{1,0:T(8,128)(2,1)S(1)} %get-tuple-element.78), kind=kOutput, calls=%fused_computation.23 | convolution fusion | flops 942667776 | bytes 4399104 | tf_op jit(solution)/shard_map/dot_general | solution.py:24
  142.0 4.4 %convert_bitcast_fusion.1 = (bf16[1,2048,512]{1,2,0:T(8,128)(2,1)}, f32[2048]{0:T(1024)S(1)}) fusion(bf16[448,2048]{1,0:T(8,128)(2,1)} %bitcast.11, bf16[448,512]{1,0:T(8,128)(2,1)S(1)} %get-tuple-element.79), kind=kOutput, calls=%fused_computation.22 | convolution fusion | flops 942667776 | bytes 4399104 | tf_op jit(solution)/shard_map/dot_general | solution.py:27
  146.3 10.9 %all-reduce.2 = (bf16[1,448]{1,0:T(2,128)(2,1)S(1)}, f32[1,2048]{1,0:T(1,128)}, f32[1,2048]{1,0:T(1,128)}) all-reduce(f32[1,448]{1,0:T(1,128)S(1)} %bitcast.75, f32[1,2048]{1,0:T(1,128)S(1)} %bitcast.70, f32[1,2048]{1,0:T(1,128)S(1)} %bitcast.71), channel_id=1, replica_groups=mesh['ep'=8,'tp'=4] {'tp'}, use_global_device_ids=true, to_apply=%region_8.9 | all-reduce | flops 4544 | bytes 35456 | tf_op jit(solution)/shard_map/psum | solution.py:111
  157.9 4.7 %all-to-all-start.4 = ((bf16[1,8,56]{2,0,1:T(2,128)(2,1)}), bf16[1,8,56]{2,0,1:T(2,128)(2,1)S(1)}, u32[]{:S(2)}, u32[]{:S(2)}) async-start(bf16[1,8,56]{2,0,1:T(2,128)(2,1)} %reshape.231), calls=%async_computation.5 | async-start | bytes 8192 | tf_op jit(solution)/shard_map/all_to_all | solution.py:116
  162.6 4.9 %multiply_reduce_fusion = (f32[512]{0:T(512)}, bf16[1,512,2048]{2,1,0:T(8,128)(2,1)}) fusion(bf16[448,512]{1,0:T(8,128)(2,1)} %get-tuple-element.67, bf16[448,2048]{1,0:T(8,128)(2,1)} %bitcast.7, f32[448]{0:T(512)S(1)} %copy-done.9), kind=kOutput, calls=%fused_computation.7 | convolution fusion | flops 945421824 | bytes 4394752 | tf_op jit(solution)/shard_map/dot_general | solution.py:23
  167.6 3.9 %copy.90 = bf16[1,2048,512]{2,1,0:T(8,128)(2,1)} copy(bf16[1,2048,512]{1,2,0:T(8,128)(2,1)} %get-tuple-element.76) | data formatting | bytes 4194304
  171.5 3.9 %copy.91 = bf16[1,2048,512]{2,1,0:T(8,128)(2,1)} copy(bf16[1,2048,512]{1,2,0:T(8,128)(2,1)} %get-tuple-element.74) | data formatting | bytes 4194304
  177.7 2.0 convert_element_type.94
  179.7 6.0 %all-to-all-start.3 = ((bf16[1,8,56,512]{3,2,0,1:T(8,128)(2,1)}), bf16[1,8,56,512]{3,2,0,1:T(8,128)(2,1)S(1)}, u32[]{:S(2)}, u32[]{:S(2)}) async-start(bf16[1,8,56,512]{3,2,0,1:T(8,128)(2,1)} %bitcast.16), calls=%async_computation.4 | async-start | bytes 917504 | tf_op jit(solution)/shard_map/all_to_all | solution.py:115
  185.9 34.9 %all-gather = f32[4096,8]{0,1:T(8,128)S(1)} all-gather(f32[512,8]{0,1:T(8,128)S(1)} %fusion.15), channel_id=2, replica_groups=mesh['ep'=8,'tp'=4] {'ep'}, dimensions={0}, use_global_device_ids=true | all-gather | bytes 147456 | tf_op jit(solution)/shard_map/all_gather | solution.py:43
  224.4 7.0 %all_gather.9 = bf16[128,2048]{1,0:T(8,128)(2,1)S(1)} all-gather(bf16[128,512]{1,0:T(8,128)(2,1)S(1)} %fusion.11), channel_id=1, replica_groups=mesh['ep'=8,'tp'=4] {'tp'}, dimensions={1}, use_global_device_ids=true | all-gather | bytes 655360 | tf_op jit(solution)/shard_map/all_gather | solution.py:140
  (81 shorter events, 21.3 us)
Async XLA Ops:
  7.2 81.6 %copy-start = (bf16[1,2048,512]{2,1,0:T(8,128)(2,1)S(1)}, bf16[1,2048,512]{2,1,0:T(8,128)(2,1)}, u32[]{:S(2)}) copy-start(bf16[1,2048,512]{2,1,0:T(8,128)(2,1)} %param.10) | copy-start | bytes 6291460
  11.0 1.4 copy-start.6
  14.0 1.6 copy-start.4
  14.0 13.7 %copy-start.1 = (bf16[128,2048]{1,0:T(8,128)(2,1)S(1)}, bf16[128,2048]{1,0:T(8,128)(2,1)}, u32[]{:S(2)}) copy-start(bf16[128,2048]{1,0:T(8,128)(2,1)} %param.7) | copy-start | bytes 1572868
  20.4 13.7 %all-to-all-start = ((bf16[1,8,56]{2,0,1:T(2,128)(2,1)}), bf16[1,8,56]{2,0,1:T(2,128)(2,1)S(1)}, u32[]{:S(2)}, u32[]{:S(2)}) async-start(bf16[1,8,56]{2,0,1:T(2,128)(2,1)} %reshape.230), calls=%async_computation | async-start | bytes 8192 | tf_op jit(solution)/shard_map/all_to_all | solution.py:84
  34.1 45.8 %all-to-all-start.2 = ((bf16[1,8,56,2048]{3,2,0,1:T(8,128)(2,1)}), bf16[1,8,56,2048]{3,2,0,1:T(8,128)(2,1)}, u32[]{:S(2)}, u32[]{:S(2)}) async-start(bf16[1,8,56,2048]{3,2,0,1:T(8,128)(2,1)} %bitcast.68), calls=%async_computation.2 | async-start | bytes 3670016 | tf_op jit(solution)/shard_map/all_to_all | solution.py:82
  79.9 46.5 %all-to-all-start.1 = ((bf16[1,8,56,2048]{3,2,0,1:T(8,128)(2,1)}), bf16[1,8,56,2048]{3,2,0,1:T(8,128)(2,1)}, u32[]{:S(2)}, u32[]{:S(2)}) async-start(bf16[1,8,56,2048]{3,2,0,1:T(8,128)(2,1)} %bitcast.67), calls=%async_computation.1 | async-start | bytes 3670016 | tf_op jit(solution)/shard_map/all_to_all | solution.py:83
  84.2 93.5 %reduce-scatter.2.cloned.1.call-start = ((), (), s32[]{:S(2)}) async-start(), calls=%async_computation.6 | async-start | bytes 4587520 | tf_op jit(solution)/shard_map/reduce_scatter | solution.py:110
  84.6 41.8 %copy-start.8 = (f32[448]{0:T(512)}, f32[448]{0:T(512)S(1)}, u32[]{:S(2)}) copy-start(f32[448]{0:T(512)S(1)} %reshape.164) | copy-start | bytes 5380
  131.9 1.6 copy-start.2
  142.0 4.4 %copy-start.5 = (f32[2048]{0:T(1024)S(1)}, f32[2048]{0:T(1024)}, u32[]{:S(2)}) copy-start(f32[2048]{0:T(1024)} %get-tuple-element.77) | copy-start | bytes 24580
  142.0 4.4 %copy-start.10 = (f32[448]{0:T(512)S(1)}, f32[448]{0:T(512)}, u32[]{:S(2)}) copy-start(f32[448]{0:T(512)} %get-tuple-element.66) | copy-start | bytes 5380
  142.0 20.7 %copy-start.9 = (f32[448]{0:T(512)S(1)}, f32[448]{0:T(512)}, u32[]{:S(2)}) copy-start(f32[448]{0:T(512)} %copy-done.8) | copy-start | bytes 5380
  157.9 17.5 %all-to-all-start.4 = ((bf16[1,8,56]{2,0,1:T(2,128)(2,1)}), bf16[1,8,56]{2,0,1:T(2,128)(2,1)S(1)}, u32[]{:S(2)}, u32[]{:S(2)}) async-start(bf16[1,8,56]{2,0,1:T(2,128)(2,1)} %reshape.231), calls=%async_computation.5 | async-start | bytes 8192 | tf_op jit(solution)/shard_map/all_to_all | solution.py:116
  175.4 10.3 %copy-start.7 = (f32[128,2]{0,1:T(2,128)S(1)}, f32[128,2]{0,1:T(2,128)}, u32[]{:S(2)}) copy-start(f32[128,2]{0,1:T(2,128)} %get-tuple-element.69) | copy-start | bytes 3076
  179.7 41.7 %all-to-all-start.3 = ((bf16[1,8,56,512]{3,2,0,1:T(8,128)(2,1)}), bf16[1,8,56,512]{3,2,0,1:T(8,128)(2,1)S(1)}, u32[]{:S(2)}, u32[]{:S(2)}) async-start(bf16[1,8,56,512]{3,2,0,1:T(8,128)(2,1)} %bitcast.16), calls=%async_computation.4 | async-start | bytes 917504 | tf_op jit(solution)/shard_map/all_to_all | solution.py:115
  220.8 3.7 %copy-start.3 = (f32[512,8]{0,1:T(8,128)}, f32[512,8]{0,1:T(8,128)S(1)}, u32[]{:S(2)}) copy-start(f32[512,8]{0,1:T(8,128)S(1)} %reduce_sum.114) | copy-start | bytes 49156
Sparse Core Ops, SparseCore 0:
  136.7 40.2 reduce-scatter.1
